TPU v7x, 128 devices: a whole 4x4x4 slice. The times are simulated.
128 devices in a mesh: ep: 64 (over z, y, x), tp: 2 (over core).
Axes of the slice: x: 4, y: 4, z: 4, core: 2. Of those that a mesh axis runs over, the one named last changes fastest.
Arguments:
- stream: bfloat16 [4096, 2048], P('ep', 'tp'), may hold values from -40 to 40
- conv_state: bfloat16 [4096, 3, 2048], P('ep', None, 'tp'), may hold values from -5 to 5
- recur_state: float32 [4096, 2048], P('ep', 'tp'), may hold values from -5 to 5
- mix_gain: float32 [2048], replicated, may hold values from 0.1 to 1.9
- branch_weight: bfloat16 [2048, 2048], P(None, 'tp'), may hold values from -0.125 to 0.125
- gate_weight: bfloat16 [2048, 2048], P(None, 'tp'), may hold values from -0.125 to 0.125
- conv_taps: float32 [4, 2048], P(None, 'tp'), may hold values from -3 to 3
- recur_map: bfloat16 [16, 128, 128], P('tp'), may hold values from -0.5 to 0.5
- input_map: bfloat16 [16, 128, 128], P('tp'), may hold values from -0.5 to 0.5
- decay_logit: float32 [2048], P('tp'), may hold values from -1 to 6
- out_weight: bfloat16 [2048, 2048], P(None, 'tp'), may hold values from -0.125 to 0.125
- moe_gain: float32 [2048], replicated, may hold values from 0.1 to 1.9
- route_ids: int32 [4096, 6], P('ep'), may hold values from 0 to 63, all different within a row; in each aligned block of 64 rows (0 to 63, 64 to 127, ...) at most 18 rows name the same one
- route_weights: float32 [4096, 6], P('ep'), may hold values from 0.2 to 1
- expert_gate: bfloat16 [64, 2048, 512], P('ep', None, 'tp'), may hold values from -0.125 to 0.125
- expert_up: bfloat16 [64, 2048, 512], P('ep', None, 'tp'), may hold values from -0.125 to 0.125
- expert_down: bfloat16 [64, 512, 2048], P('ep', None, 'tp'), may hold values from -0.25 to 0.25
- dense_gate: bfloat16 [2048, 512], P(None, 'tp'), may hold values from -0.125 to 0.125
- dense_up: bfloat16 [2048, 512], P(None, 'tp'), may hold values from -0.125 to 0.125
- dense_down: bfloat16 [512, 2048], P(None, 'tp'), may hold values from -0.25 to 0.25
- dense_scale: float32 [2048], P('tp'), may hold values from 0.1 to 1.9
Outputs:
- result: bfloat16 [4096, 2048], P('ep', 'tp')
- new_state: float32 [4096, 2048], P('ep', 'tp')
- new_conv: bfloat16 [4096, 3, 2048], P('ep', None, 'tp')
Inputs may be any that keep to these rules, and one draw needn't show every extreme that they name: `route_ids`: each row names 6 different experts; among the rows of one index of ep no expert is named by more than 18 rows, and in every draw some expert is named by exactly 18 rows of some index.
All inputs are finite; a program needn't handle non-finite values.
Results may differ from a plain program's by a relative error of at most 0.014.
Values may be sent and summed in bfloat16 or wider, within the bound.
No kernel may reach another device: no remote copies, remote signals or barrier semaphores. Data moves between devices by JAX's collectives and lax.ppermute only.
A program may use at most 128 MiB of HBM per device.

v0:
```python
import jax
import jax.numpy as jnp
from jax import lax
from jax.sharding import PartitionSpec as P


def laid_out(tiles, dim):
    shape = list(tiles.shape[1:])
    shape[dim] *= tiles.shape[0]
    return jnp.moveaxis(tiles, 0, dim).reshape(shape)


def sent_to_all(shard, axis):
    length = lax.axis_size(axis)
    return lax.all_to_all(
        jnp.broadcast_to(shard[None], (length, *shard.shape)), axis, 0, 0, tiled=True
    )


def gathered_copies(shard, axis, dim):
    return laid_out(sent_to_all(shard, axis), dim)


def accumulate_with(weight, segment):
    return jnp.dot(segment, weight, preferred_element_type=jnp.float32)


def normalize(part_rows, gain_vec):
    whole_rows = gathered_copies(part_rows, "tp", 1).astype(jnp.float32)
    row_mean = jnp.mean(whole_rows, axis=1, keepdims=True)
    row_var = jnp.mean(whole_rows * whole_rows, axis=1, keepdims=True) - row_mean * row_mean
    return ((whole_rows - row_mean) * lax.rsqrt(row_var + 1e-05) * gain_vec).astype(jnp.bfloat16)


def per_device(
    stream,
    conv_state,
    recur_state,
    mix_gain,
    branch_weight,
    gate_weight,
    conv_taps,
    recur_map,
    input_map,
    decay_logit,
    out_weight,
    moe_gain,
    route_ids,
    route_weights,
    expert_gate,
    expert_up,
    expert_down,
    dense_gate,
    dense_up,
    dense_down,
    dense_scale,
):
    seq_count = stream.shape[0]
    out_width = stream.shape[1]
    normed = normalize(stream, mix_gain)
    branch_in = jnp.dot(normed, branch_weight, preferred_element_type=jnp.float32).astype(
        jnp.bfloat16
    )
    gate_pre = jnp.dot(normed, gate_weight, preferred_element_type=jnp.float32).astype(jnp.bfloat16)
    conv_sum = branch_in.astype(jnp.float32) * conv_taps[3]
    for offset in range(3):
        conv_sum = conv_sum + conv_state[:, offset].astype(jnp.float32) * conv_taps[offset]
    conv_out = conv_sum.astype(jnp.bfloat16)
    new_conv = jnp.concatenate([conv_state[:, 1:], branch_in[:, None]], axis=1)
    block_count = recur_map.shape[0]
    block_width = recur_map.shape[1]
    grouped = conv_out.reshape(seq_count, block_count, block_width)
    recur_gate = jax.nn.sigmoid(
        jnp.einsum("nbc,bcd->nbd", grouped, recur_map, preferred_element_type=jnp.float32)
    ).reshape(seq_count, -1)
    input_gate = jax.nn.sigmoid(
        jnp.einsum("nbc,bcd->nbd", grouped, input_map, preferred_element_type=jnp.float32)
    ).reshape(seq_count, -1)
    log_decay = -8.0 * recur_gate * jax.nn.softplus(-decay_logit)
    driven = jnp.sqrt(-jnp.expm1(2.0 * log_decay)) * (input_gate * conv_out.astype(jnp.float32))
    new_state = jnp.exp(log_decay) * recur_state + driven
    mixer_in = (jax.nn.gelu(gate_pre.astype(jnp.float32)) * new_state).astype(jnp.bfloat16)
    mixer_out = accumulate_with(
        out_weight, lax.all_gather(mixer_in, "tp", axis=1, tiled=True)
    ).astype(jnp.bfloat16)
    resid = (stream.astype(jnp.float32) + mixer_out.astype(jnp.float32)).astype(jnp.bfloat16)
    normed_two = normalize(resid, moe_gain)
    top_count = route_ids.shape[1]
    expert_count = lax.axis_size("ep")
    capacity = max(2, min(seq_count, 3 * seq_count * top_count // expert_count))
    flat_ids = route_ids.reshape(-1)
    one_hot = (flat_ids[:, None] == jnp.arange(expert_count, dtype=jnp.int32)[None, :]).astype(
        jnp.int32
    )
    slot_rank = jnp.sum(one_hot * (jnp.cumsum(one_hot, axis=0) - 1), axis=1)
    slot_index = (flat_ids * capacity + slot_rank).reshape(seq_count, top_count)
    dispatch_table = jnp.sum(
        (
            slot_index[:, :, None]
            == jnp.arange(expert_count * capacity, dtype=jnp.int32)[None, None, :]
        ).astype(jnp.bfloat16),
        axis=1,
    )
    own_gate = expert_gate[0]
    own_up = expert_up[0]
    own_down = expert_down[0]
    own_features = lax.dynamic_slice_in_dim(
        normed_two, lax.axis_index("tp") * out_width, out_width, 1
    )
    outgoing = lax.dot_general(
        dispatch_table, own_features, (((0,), (0,)), ((), ())), preferred_element_type=jnp.float32
    )
    outgoing = outgoing.astype(jnp.bfloat16).reshape(expert_count, capacity, -1)
    incoming = lax.all_gather(
        lax.all_to_all(outgoing, "ep", split_axis=0, concat_axis=0, tiled=True),
        "tp",
        axis=2,
        tiled=True,
    )
    source_count, slot_count, feature_count = incoming.shape
    taken_rows = incoming.reshape(source_count * slot_count, feature_count)
    gate_sum = jnp.dot(taken_rows, own_gate, preferred_element_type=jnp.float32)
    up_sum = jnp.dot(taken_rows, own_up, preferred_element_type=jnp.float32)
    hidden = (jax.nn.silu(gate_sum) * up_sum).astype(jnp.bfloat16)
    served_rows = accumulate_with(own_down, gathered_copies(hidden, "tp", 1))
    served = served_rows.astype(jnp.bfloat16).reshape(source_count, slot_count, -1)
    returned = lax.all_to_all(served, "ep", split_axis=0, concat_axis=0, tiled=True).reshape(
        expert_count * capacity, -1
    )
    picked = returned[slot_index]
    routed = jnp.sum(picked.astype(jnp.float32) * route_weights[:, :, None], axis=1)
    dense_gsum = jnp.dot(normed_two, dense_gate, preferred_element_type=jnp.float32)
    dense_usum = jnp.dot(normed_two, dense_up, preferred_element_type=jnp.float32)
    dense_hidden = (jax.nn.silu(dense_gsum) * dense_usum).astype(jnp.bfloat16)
    dense_out = accumulate_with(
        dense_down, lax.all_gather(dense_hidden, "tp", axis=1, tiled=True)
    ).astype(jnp.bfloat16)
    result = (
        resid.astype(jnp.float32) + routed + dense_scale * dense_out.astype(jnp.float32)
    ).astype(jnp.bfloat16)
    return (result, new_state, new_conv)


def solution(mesh):
    in_specs = (
        P("ep", "tp"),
        P("ep", None, "tp"),
        P("ep", "tp"),
        P(),
        P(None, "tp"),
        P(None, "tp"),
        P(None, "tp"),
        P("tp", None, None),
        P("tp", None, None),
        P("tp"),
        P(None, "tp"),
        P(),
        P("ep", None),
        P("ep", None),
        P("ep", None, "tp"),
        P("ep", None, "tp"),
        P("ep", None, "tp"),
        P(None, "tp"),
        P(None, "tp"),
        P(None, "tp"),
        P("tp"),
    )
    out_specs = (P("ep", "tp"), P("ep", "tp"), P("ep", None, "tp"))
    return jax.shard_map(
        per_device, mesh=mesh, in_specs=in_specs, out_specs=out_specs, check_vma=False
    )
```

profile of v0, /device:TPU:0, one launch (start us, length us, event | category | flops | bytes accessed | tf_op | source)
XLA Modules:
  0.0 197.2 jit_solution(7304002262852420736)
XLA Ops:
  7.2 1.7 broadcast_in_dim.10
  8.9 3.4 %all-to-all-start = ((bf16[2,64,1024]{2,1,0:T(8,128)(2,1)}), bf16[2,64,1024]{2,1,0:T(8,128)(2,1)S(1)}, u32[]{:S(2)}, u32[]{:S(2)}) async-start(bf16[2,64,1024]{2,1,0:T(8,128)(2,1)} %broadcast_in_dim.10), calls=%async_computation | async-start | bytes 524288 | tf_op jit(solution)/shard_map/all_to_all | solution.py:15
  12.4 0.9 fusion.51
  13.3 0.7 all-to-all-done
  14.0 0.2 convert_reduce_fusion.1
  14.3 4.0 %fusion.38 = (bf16[64,1024]{1,0:T(8,128)(2,1)S(1)}, bf16[64,1024]{1,0:T(8,128)(2,1)}) fusion(f32[1024]{0:T(1024)S(1)} %bitcast.101, bf16[64,3,1024]{2,0,1:T(8,128)(2,1)S(1)} %copy-done.6, f32[1024]{0:T(1024)S(1)} %bitcast.102, f32[1024]{0:T(1024)S(1)} %bitcast.100, f32[1024]{0:T(1024)S(1)} %bitcast.99, bf16[2048,1024]{1,0:T(8,128)(2,1)} %param.25, ...), kind=kOutput, calls=%fused_computation.64 | convolution fusion | flops 269811712 | bytes 5399040 | tf_op jit(solution)/shard_map/dot_general | solution.py:61
  18.2 0.2 fusion.5
  18.5 0.2 fusion.9
  18.7 0.2 copy-done.19
  18.9 0.3 copy-done.13
  19.2 0.2 fusion.36
  19.5 1.0 fusion.34
  20.5 2.1 %all_gather.9 = bf16[64,2048]{1,0:T(8,128)(2,1)S(1)} all-gather(bf16[64,1024]{1,0:T(8,128)(2,1)S(1)} %fusion.34), channel_id=1, replica_groups=mesh['ep'=64,'tp'=2] {'tp'}, dimensions={1}, use_global_device_ids=true | all-gather | bytes 393216 | tf_op jit(solution)/shard_map/all_gather | solution.py:84
  22.6 0.9 fusion.15
  23.5 0.7 broadcast_in_dim.11
  24.2 3.4 %all-to-all-start.1 = ((bf16[2,64,1024]{2,1,0:T(8,128)(2,1)}), bf16[2,64,1024]{2,1,0:T(8,128)(2,1)S(1)}, u32[]{:S(2)}, u32[]{:S(2)}) async-start(bf16[2,64,1024]{2,1,0:T(8,128)(2,1)} %broadcast_in_dim.11), calls=%async_computation.1 | async-start | bytes 524288 | tf_op jit(solution)/shard_map/all_to_all | solution.py:15
  27.8 0.1 eq.38
  27.9 0.1 eq.42
  28.1 1.1 all-to-all-done.1
  29.3 0.9 reduce-window.6
  30.2 0.2 slice_reduce_fusion
  30.8 1.0 fusion.23
  31.8 0.2 convert_reduce_fusion
  32.2 0.7 copy-done.4
  32.9 1.7 convolution_convert_fusion.1
  34.6 2.4 %reshape.118 = bf16[64,18,1024]{2,1,0:T(8,128)(2,1)} reshape(bf16[1152,1024]{1,0:T(8,128)(2,1)S(1)} %convolution_convert_fusion.1) | data formatting | bytes 4718592 | tf_op jit(solution)/shard_map/reshape | solution.py:113
  37.0 53.3 %all_to_all.25 = bf16[64,18,1024]{2,1,0:T(8,128)(2,1)} all-to-all(bf16[64,18,1024]{2,1,0:T(8,128)(2,1)} %reshape.118), channel_id=1, replica_groups=mesh['ep'=64,'tp'=2] {'ep'}, dimensions={0} | all-to-all | bytes 4718592 | tf_op jit(solution)/shard_map/all_to_all | solution.py:115
  90.3 15.6 %all-gather.2.cloned.1.call-done = bf16[64,18,2048]{2,1,0:T(8,128)(2,1)} async-done(((bf16[64,18,1024]{2,1,0:T(8,128)(2,1)}), bf16[64,18,2048]{2,1,0:T(8,128)(2,1)}) %all-gather.2.cloned.1.call-update) | async-done | bytes 4718608 | tf_op jit(solution)/shard_map/all_gather | solution.py:114
  106.0 7.8 %reshape.119 = bf16[1152,2048]{1,0:T(8,128)(2,1)} reshape(bf16[64,18,2048]{2,1,0:T(8,128)(2,1)} %all-gather.2.cloned.1.call-done) | data formatting | bytes 9437184 | tf_op jit(solution)/shard_map/reshape | solution.py:121
  113.7 3.9 %fusion.21 = f32[1152,256]{1,0:T(8,128)S(1)} fusion(bf16[1152,2048]{1,0:T(8,128)(2,1)} %reshape.119, bf16[1,2048,256]{2,1,0:T(8,128)(2,1)S(1)} %copy-done.20), kind=kOutput, calls=%fused_computation.34 | convolution fusion | flops 1207959552 | bytes 6946816 | tf_op jit(solution)/shard_map/dot_general | solution.py:122
  117.7 0.1 copy-done.21
  117.8 1.6 fusion
  119.4 0.3 copy.78
  119.8 4.7 %all_to_all.26 = bf16[2,1152,256]{1,2,0:T(8,128)(2,1)S(1)} all-to-all(bf16[2,1152,256]{1,2,0:T(8,128)(2,1)S(1)} %broadcast_in_dim.12), channel_id=1, replica_groups=mesh['ep'=64,'tp'=2] {'tp'}, dimensions={0} | all-to-all | bytes 2359296 | tf_op jit(solution)/shard_map/all_to_all | solution.py:15
  124.4 1.4 convolution_convert_fusion
  125.9 2.4 %reshape.121 = bf16[64,18,1024]{2,1,0:T(8,128)(2,1)} reshape(bf16[1152,1024]{1,0:T(8,128)(2,1)S(1)} %convolution_convert_fusion) | data formatting | bytes 4718592 | tf_op jit(solution)/shard_map/reshape | solution.py:126
  128.3 10.8 %all-to-all-start.4 = ((bf16[64,18,1024]{2,1,0:T(8,128)(2,1)}), bf16[64,18,1024]{2,1,0:T(8,128)(2,1)}, u32[]{:S(2)}, u32[]{:S(2)}) async-start(bf16[64,18,1024]{2,1,0:T(8,128)(2,1)} %reshape.121), calls=%async_computation.4 | async-start | bytes 6291456 | tf_op jit(solution)/shard_map/all_to_all | solution.py:127
  139.3 0.7 copy.80
  140.1 0.3 fusion.52
  140.4 1.5 fusion.18
  141.9 2.0 %all_gather.11 = bf16[64,512]{1,0:T(8,128)(2,1)} all-gather(bf16[64,256]{1,0:T(8,128)(2,1)S(1)} %fusion.18), channel_id=1, replica_groups=mesh['ep'=64,'tp'=2] {'tp'}, dimensions={1}, use_global_device_ids=true | all-gather | bytes 98304 | tf_op jit(solution)/shard_map/all_gather | solution.py:136
  143.9 0.8 pad_maximum_fusion
  144.7 36.2 %all-to-all-done.4 = bf16[64,18,1024]{2,1,0:T(8,128)(2,1)} async-done(((bf16[64,18,1024]{2,1,0:T(8,128)(2,1)}), bf16[64,18,1024]{2,1,0:T(8,128)(2,1)}, u32[]{:S(2)}, u32[]{:S(2)}) %all-to-all-start.4) | async-done | bytes 2359328 | tf_op jit(solution)/shard_map/all_to_all | solution.py:127
  180.9 2.9 %reshape.122 = bf16[1152,1024]{1,0:T(8,128)(2,1)S(1)} reshape(bf16[64,18,1024]{2,1,0:T(8,128)(2,1)} %all-to-all-done.4) | data formatting | bytes 4718592 | tf_op jit(solution)/shard_map/reshape | solution.py:127
  183.8 2.7 %gather_fusion = bf16[384,1024]{1,0:T(8,128)(2,1)} fusion(bf16[1152,1024]{1,0:T(8,128)(2,1)S(1)} %reshape.122, s32[1024]{0:T(1024)S(1)} %pad_clamp_fusion), kind=kCustom, calls=%fused_computation | custom fusion | bytes 1574400 | tf_op jit(solution)/shard_map/gather | solution.py:130
  186.5 1.3 reshape.138
  187.8 1.6 multiply_reduce_fusion
  189.4 1.0 fusion.17
  (67 shorter events, 1.3 us)
Async XLA Ops:
  7.2 117.3 %copy-start = (bf16[1,512,1024]{2,1,0:T(8,128)(2,1)S(1)}, bf16[1,512,1024]{2,1,0:T(8,128)(2,1)}, u32[]{:S(2)}) copy-start(bf16[1,512,1024]{2,1,0:T(8,128)(2,1)} %param.37) | copy-start | bytes 3145732
  7.2 7.0 %copy-start.6 = (bf16[64,3,1024]{2,0,1:T(8,128)(2,1)S(1)}, bf16[64,3,1024]{2,0,1:T(8,128)(2,1)}, u32[]{:S(2)}) copy-start(bf16[64,3,1024]{2,0,1:T(8,128)(2,1)} %param.22) | copy-start | bytes 1179652
  7.2 7.0 %copy-start.14 = (f32[2048]{0:T(1024)S(1)}, f32[2048]{0:T(1024)}, u32[]{:S(2)}) copy-start(f32[2048]{0:T(1024)} %param.24) | copy-start | bytes 24580
  8.9 5.0 %all-to-all-start = ((bf16[2,64,1024]{2,1,0:T(8,128)(2,1)}), bf16[2,64,1024]{2,1,0:T(8,128)(2,1)S(1)}, u32[]{:S(2)}, u32[]{:S(2)}) async-start(bf16[2,64,1024]{2,1,0:T(8,128)(2,1)} %broadcast_in_dim.10), calls=%async_computation | async-start | bytes 524288 | tf_op jit(solution)/shard_map/all_to_all | solution.py:15
  14.2 4.0 %copy-start.22 = (bf16[8,128,128]{2,1,0:T(8,128)(2,1)S(1)}, bf16[8,128,128]{2,1,0:T(8,128)(2,1)}, u32[]{:S(2)}) copy-start(bf16[8,128,128]{2,1,0:T(8,128)(2,1)} %param.29) | copy-start | bytes 786436
  14.2 4.2 %copy-start.23 = (bf16[8,128,128]{2,1,0:T(8,128)(2,1)S(1)}, bf16[8,128,128]{2,1,0:T(8,128)(2,1)}, u32[]{:S(2)}) copy-start(bf16[8,128,128]{2,1,0:T(8,128)(2,1)} %param.28) | copy-start | bytes 786436
  14.3 5.2 %copy-start.3 = (bf16[2048,1024]{1,0:T(8,128)(2,1)S(1)}, bf16[2048,1024]{1,0:T(8,128)(2,1)}, u32[]{:S(2)}) copy-start(bf16[2048,1024]{1,0:T(8,128)(2,1)} %param.26) | copy-start | bytes 12582916
  18.2 0.7 copy-start.19
  18.2 1.0 copy-start.13
  19.4 1.0 copy-start.9
  19.4 3.1 %copy-start.2 = (bf16[2048,1024]{1,0:T(8,128)(2,1)S(1)}, bf16[2048,1024]{1,0:T(8,128)(2,1)}, u32[]{:S(2)}) copy-start(bf16[2048,1024]{1,0:T(8,128)(2,1)} %param.31) | copy-start | bytes 12582916
  19.5 3.1 %copy-start.10 = (bf16[64,1024]{1,0:T(8,128)(2,1)S(1)}, bf16[64,1024]{1,0:T(8,128)(2,1)}, u32[]{:S(2)}) copy-start(bf16[64,1024]{1,0:T(8,128)(2,1)} %param.21) | copy-start | bytes 393220
  22.6 5.1 %copy-start.15 = (s32[64,6]{0,1:T(8,128)S(1)}, s32[64,6]{0,1:T(8,128)}, u32[]{:S(2)}) copy-start(s32[64,6]{0,1:T(8,128)} %param.33) | copy-start | bytes 4612
  23.4 8.6 %copy-start.16 = (f32[2048]{0:T(1024)S(1)}, f32[2048]{0:T(1024)}, u32[]{:S(2)}) copy-start(f32[2048]{0:T(1024)} %param.32) | copy-start | bytes 24580
  24.2 5.0 %all-to-all-start.1 = ((bf16[2,64,1024]{2,1,0:T(8,128)(2,1)}), bf16[2,64,1024]{2,1,0:T(8,128)(2,1)S(1)}, u32[]{:S(2)}, u32[]{:S(2)}) async-start(bf16[2,64,1024]{2,1,0:T(8,128)(2,1)} %broadcast_in_dim.11), calls=%async_computation.1 | async-start | bytes 524288 | tf_op jit(solution)/shard_map/all_to_all | solution.py:15
  27.6 78.3 %all-gather.2.cloned.1.call-start = ((), (), s32[]{:S(2)}) async-start(), calls=%async_computation.5 | async-start | bytes 9437184 | tf_op jit(solution)/shard_map/all_gather | solution.py:114
  32.1 0.7 copy-start.4
  90.3 23.4 %copy-start.20 = (bf16[1,2048,256]{2,1,0:T(8,128)(2,1)S(1)}, bf16[1,2048,256]{2,1,0:T(8,128)(2,1)}, u32[]{:S(2)}) copy-start(bf16[1,2048,256]{2,1,0:T(8,128)(2,1)} %param.35) | copy-start | bytes 3145732
  113.7 3.9 %copy-start.1 = (bf16[1152,2048]{1,0:T(8,128)(2,1)S(1)}, bf16[1152,2048]{1,0:T(8,128)(2,1)}, u32[]{:S(2)}) copy-start(bf16[1152,2048]{1,0:T(8,128)(2,1)} %reshape.119) | copy-start | bytes 14155780
  113.7 4.1 %copy-start.21 = (bf16[1,2048,256]{2,1,0:T(8,128)(2,1)S(1)}, bf16[1,2048,256]{2,1,0:T(8,128)(2,1)}, u32[]{:S(2)}) copy-start(bf16[1,2048,256]{2,1,0:T(8,128)(2,1)} %param.36) | copy-start | bytes 3145732
  128.3 11.0 %copy-start.18 = (f32[64,6]{0,1:T(8,128)S(1)}, f32[64,6]{0,1:T(8,128)}, u32[]{:S(2)}) copy-start(f32[64,6]{0,1:T(8,128)} %param.34) | copy-start | bytes 4612
  128.3 11.7 %copy-start.5 = (bf16[64,2048]{1,0:T(8,128)(2,1)S(1)}, bf16[64,2048]{1,0:T(8,128)(2,1)}, u32[]{:S(2)}) copy-start(bf16[64,2048]{1,0:T(8,128)(2,1)} %copy-done.4) | copy-start | bytes 786436
  128.3 11.7 %copy-start.7 = (bf16[2048,256]{1,0:T(8,128)(2,1)S(1)}, bf16[2048,256]{1,0:T(8,128)(2,1)}, u32[]{:S(2)}) copy-start(bf16[2048,256]{1,0:T(8,128)(2,1)} %param.38) | copy-start | bytes 3145732
  128.3 52.5 %all-to-all-start.4 = ((bf16[64,18,1024]{2,1,0:T(8,128)(2,1)}), bf16[64,18,1024]{2,1,0:T(8,128)(2,1)}, u32[]{:S(2)}, u32[]{:S(2)}) async-start(bf16[64,18,1024]{2,1,0:T(8,128)(2,1)} %reshape.121), calls=%async_computation.4 | async-start | bytes 6291456 | tf_op jit(solution)/shard_map/all_to_all | solution.py:127
  139.1 4.8 %slice-start = ((bf16[64,3,1024]{2,0,1:T(8,128)(2,1)}), bf16[64,2,1024]{2,0,1:T(8,128)(2,1)S(1)}, s32[]{:S(2)}) async-start(bf16[64,3,1024]{2,0,1:T(8,128)(2,1)} %param.22), calls=%async_computation.6 | async-start | bytes 524288 | tf_op jit(solution)/shard_map/slice | solution.py:69
  139.1 4.8 %copy-start.11 = (bf16[64,1024]{1,0:T(8,128)(2,1)S(1)}, bf16[64,1024]{1,0:T(8,128)(2,1)}, u32[]{:S(2)}) copy-start(bf16[64,1024]{1,0:T(8,128)(2,1)} %get-tuple-element.18) | copy-start | bytes 393220
  186.5 2.9 %copy-start.17 = (f32[1024]{0:T(1024)S(1)}, f32[1024]{0:T(1024)}, u32[]{:S(2)}) copy-start(f32[1024]{0:T(1024)} %param.41) | copy-start | bytes 12292
  187.8 1.6 copy-start.8
  187.8 1.6 copy-start.12
Sparse Core Ops, SparseCore 0:
  90.4 15.4 all-gather.1
where the time goes:
time: 198 us; the launch traced here: 197 us
  blocking collectives  62.1 us (31%)
  waiting for transfers between devices  53.6 us (27%)
  local copies, waits for them, and re-layouts  26.5 us (13%)
  starting transfers between devices  17.7 us (9%)
  matrix products  17.6 us (9%)
  between operations  14.5 us (7%)
  other arithmetic  5.26 us (3%)
    all_to_all x1, blocking collectives, per_device(): lax.all_to_all(outgoing, 'ep', split_axis=0, concat_axis=0, tiled=True)  53.3 us
    all_to_all x1, waiting for transfers between devices, per_device(): lax.all_to_all(served, 'ep', split_axis=0, concat_axis=0, tiled=True)  36.2 us
    all_gather x1, waiting for transfers between devices, per_device(): lax.all_gather(lax.all_to_all(outgoing, 'ep', split_axis=0, concat_axis=0...  15.6 us
    all_to_all x1, starting transfers between devices, per_device(): lax.all_to_all(served, 'ep', split_axis=0, concat_axis=0, tiled=True)  10.8 us
    reshape x1, local copies, waits for them, and re-layouts, per_device(): taken_rows = incoming.reshape(source_count * slot_count, feature_count)  7.77 us
    all_to_all x2, starting transfers between devices, sent_to_all(): lax.all_to_all(jnp.broadcast_to(shard[None], (length, *shard.shape)), axi...  6.89 us
    all_to_all x1, blocking collectives, sent_to_all(): lax.all_to_all(jnp.broadcast_to(shard[None], (length, *shard.shape)), axi...  4.68 us
  transfers between devices with their start and end apart: 4, of which 4 were waited for; matrix products, arithmetic and copies ran while one was open for 2% of the time, Pallas kernels for 0%

commit v1 on v0

--- a/solution.py
+++ b/solution.py
@@ -111,11 +111,17 @@
         dispatch_table, own_features, (((0,), (0,)), ((), ())), preferred_element_type=jnp.float32
     )
     outgoing = outgoing.astype(jnp.bfloat16).reshape(expert_count, capacity, -1)
-    incoming = lax.all_gather(
-        lax.all_to_all(outgoing, "ep", split_axis=0, concat_axis=0, tiled=True),
-        "tp",
+    incoming = jnp.concatenate(
+        lax.all_to_all(
+            jnp.stack(
+                [lax.all_to_all(outgoing, "ep", split_axis=0, concat_axis=0, tiled=True)]
+                * lax.axis_size("tp")
+            ),
+            "tp",
+            0,
+            0,
+        ),
         axis=2,
-        tiled=True,
     )
     source_count, slot_count, feature_count = incoming.shape
     taken_rows = incoming.reshape(source_count * slot_count, feature_count)

time: 198 us -> 181 us (0.914)
  waiting for transfers between devices: 53.6 us -> 38.7 us
  between operations: 14.5 us -> 1.09 us
  blocking collectives: 62.1 us -> 70.6 us
  local copies, waits for them, and re-layouts: 26.5 us -> 34.4 us
  starting transfers between devices: 17.7 us -> 12.8 us
    all_gather x1 -> x0, waiting for transfers between devices: 15.6 us -> none  [per_device(): lax.all_gather(lax.all_to_all(outgoing, 'ep', split_axis=0, concat_axis=0...]
    all_to_all x0 -> x1, blocking collectives: none -> 8.61 us  [per_device(): lax.all_to_all(jnp.stack([lax.all_to_all(outgoing, 'ep', split_axis=0, co...]
    all_to_all x1, starting transfers between devices: 10.8 us -> 5.93 us  [per_device(): lax.all_to_all(served, 'ep', split_axis=0, concat_axis=0, tiled=True)]
    unnamed x50 -> x45, local copies, waits for them, and re-layouts: 2.22 us -> 5.96 us
    another operation x0 -> x1, local copies, waits for them, and re-layouts: none -> 2.63 us  [per_device(): jnp.stack([lax.all_to_all(outgoing, 'ep', split_axis=0, concat_axis=0, ti...]
    dot_general x1, matrix products: 3.9 us -> 1.41 us  [per_device(): gate_sum = jnp.dot(taken_rows, own_gate, preferred_element_type=jnp.float32)]
  transfers between devices with their start and end apart: 4 -> 3, of which waited for: 4 -> 3; matrix products, arithmetic and copies ran while one was open for 2% -> 3% of each run, Pallas kernels for 0% -> 0%
where the time goes in v1:
time: 181 us; the launch traced here: 180 us
  blocking collectives  70.6 us (39%)
  waiting for transfers between devices  38.7 us (21%)
  local copies, waits for them, and re-layouts  34.4 us (19%)
  matrix products  16.4 us (9%)
  starting transfers between devices  12.8 us (7%)
  other arithmetic  6.09 us (3%)
    all_to_all x1, blocking collectives, per_device(): lax.all_to_all(outgoing, 'ep', split_axis=0, concat_axis=0, tiled=True)  53.2 us
    all_to_all x1, waiting for transfers between devices, per_device(): lax.all_to_all(served, 'ep', split_axis=0, concat_axis=0, tiled=True)  36.9 us
    reshape x1, local copies, waits for them, and re-layouts, per_device(): jnp.concatenate(lax.all_to_all(jnp.stack([lax.all_to_all(outgoing, 'ep',...  9.36 us
    all_to_all x1, blocking collectives, per_device(): lax.all_to_all(jnp.stack([lax.all_to_all(outgoing, 'ep', split_axis=0, co...  8.61 us
    all_to_all x2, starting transfers between devices, sent_to_all(): lax.all_to_all(jnp.broadcast_to(shard[None], (length, *shard.shape)), axi...  6.89 us
    unnamed x45, local copies, waits for them, and re-layouts  5.96 us
    all_to_all x1, starting transfers between devices, per_device(): lax.all_to_all(served, 'ep', split_axis=0, concat_axis=0, tiled=True)  5.93 us
    all_to_all x1, blocking collectives, sent_to_all(): lax.all_to_all(jnp.broadcast_to(shard[None], (length, *shard.shape)), axi...  4.68 us
  transfers between devices with their start and end apart: 3, of which 3 were waited for; matrix products, arithmetic and copies ran while one was open for 3% of the time, Pallas kernels for 0%

profile of v1, /device:TPU:0, one launch (start us, length us, event | category | flops | bytes accessed | tf_op | source)
XLA Modules:
  0.0 180.1 jit_solution(7945209582787277370)
XLA Ops:
  0.7 1.7 broadcast_in_dim.10
  2.4 3.4 %all-to-all-start = ((bf16[2,64,1024]{2,1,0:T(8,128)(2,1)}), bf16[2,64,1024]{2,1,0:T(8,128)(2,1)S(1)}, u32[]{:S(2)}, u32[]{:S(2)}) async-start(bf16[2,64,1024]{2,1,0:T(8,128)(2,1)} %broadcast_in_dim.10), calls=%async_computation | async-start | bytes 524288 | tf_op jit(solution)/shard_map/all_to_all | solution.py:15
  5.9 0.9 fusion.51
  6.7 0.7 all-to-all-done
  7.5 0.2 convert_reduce_fusion.1
  7.7 4.0 %fusion.38 = (bf16[64,1024]{1,0:T(8,128)(2,1)S(1)}, bf16[64,1024]{1,0:T(8,128)(2,1)}) fusion(f32[1024]{0:T(1024)S(1)} %bitcast.111, bf16[64,3,1024]{2,0,1:T(8,128)(2,1)S(1)} %copy-done.5, f32[1024]{0:T(1024)S(1)} %bitcast.112, f32[1024]{0:T(1024)S(1)} %bitcast.110, f32[1024]{0:T(1024)S(1)} %bitcast.109, bf16[2048,1024]{1,0:T(8,128)(2,1)} %param.25, ...), kind=kOutput, calls=%fused_computation.65 | convolution fusion | flops 269811712 | bytes 5399040 | tf_op jit(solution)/shard_map/dot_general | solution.py:61
  11.7 0.2 fusion.5
  12.0 0.2 fusion.9
  12.3 0.2 fusion.36
  12.5 1.0 fusion.34
  13.5 2.1 %all_gather.6 = bf16[64,2048]{1,0:T(8,128)(2,1)S(1)} all-gather(bf16[64,1024]{1,0:T(8,128)(2,1)S(1)} %fusion.34), channel_id=1, replica_groups=mesh['ep'=64,'tp'=2] {'tp'}, dimensions={1}, use_global_device_ids=true | all-gather | bytes 393216 | tf_op jit(solution)/shard_map/all_gather | solution.py:84
  15.6 0.9 fusion.15
  16.5 0.7 broadcast_in_dim.11
  17.3 3.4 %all-to-all-start.1 = ((bf16[2,64,1024]{2,1,0:T(8,128)(2,1)}), bf16[2,64,1024]{2,1,0:T(8,128)(2,1)S(1)}, u32[]{:S(2)}, u32[]{:S(2)}) async-start(bf16[2,64,1024]{2,1,0:T(8,128)(2,1)} %broadcast_in_dim.11), calls=%async_computation.1 | async-start | bytes 524288 | tf_op jit(solution)/shard_map/all_to_all | solution.py:15
  20.8 0.1 eq.38
  21.0 0.1 eq.42
  21.1 1.1 all-to-all-done.1
  22.4 0.9 reduce-window.6
  23.3 0.2 slice_reduce_fusion
  23.9 1.0 fusion.23
  24.9 0.2 convert_reduce_fusion
  25.2 0.7 copy-done.3
  25.9 1.7 convolution_convert_fusion.1
  27.6 2.4 %reshape.118 = bf16[64,18,1024]{2,1,0:T(8,128)(2,1)} reshape(bf16[1152,1024]{1,0:T(8,128)(2,1)S(1)} %convolution_convert_fusion.1) | data formatting | bytes 4718592 | tf_op jit(solution)/shard_map/reshape | solution.py:113
  30.0 53.2 %all_to_all.30 = bf16[64,18,1024]{2,1,0:T(8,128)(2,1)S(1)} all-to-all(bf16[64,18,1024]{2,1,0:T(8,128)(2,1)} %reshape.118), channel_id=1, replica_groups=mesh['ep'=64,'tp'=2] {'ep'}, dimensions={0} | all-to-all | bytes 4718592 | tf_op jit(solution)/shard_map/all_to_all | solution.py:117
  83.2 0.9 pad_maximum_fusion
  84.1 2.6 %copy.83 = bf16[2,64,18,1024]{3,1,2,0:T(8,128)(2,1)S(1)} copy(bf16[2,64,18,1024]{3,2,1,0:T(8,128)(2,1)S(1)} %pad_maximum_fusion) | data formatting | bytes 9437184 | tf_op jit(solution)/shard_map/stack | solution.py:116
  86.8 8.6 %all_to_all.31 = bf16[2,64,18,1024]{3,1,2,0:T(8,128)(2,1)} all-to-all(bf16[2,64,18,1024]{3,1,2,0:T(8,128)(2,1)S(1)} %copy.83), channel_id=1, replica_groups=mesh['ep'=64,'tp'=2] {'tp'}, dimensions={0} | all-to-all | bytes 9437184 | tf_op jit(solution)/shard_map/all_to_all | solution.py:115
  95.4 9.4 %copy.84 = bf16[64,18,2,1024]{3,2,1,0:T(2,128)(2,1)} copy(bf16[64,18,2,1024]{3,0,1,2:T(8,128)(2,1)} %bitcast.99) | data formatting | bytes 9437184 | tf_op jit(solution)/shard_map/reshape | solution.py:114
  104.7 4.4 %copy.94 = bf16[144,8,2,1024]{3,1,2,0:T(8,128)(2,1)S(1)} copy(bf16[144,8,2,1024]{3,2,1,0:T(2,128)(2,1)} %bitcast.100) | data formatting | bytes 9437184
  109.1 1.4 fusion.21
  110.6 1.6 fusion
  112.1 0.3 copy.85
  112.5 4.7 %all_to_all.32 = bf16[2,1152,256]{1,2,0:T(8,128)(2,1)S(1)} all-to-all(bf16[2,1152,256]{1,2,0:T(8,128)(2,1)S(1)} %broadcast_in_dim.12), channel_id=1, replica_groups=mesh['ep'=64,'tp'=2] {'tp'}, dimensions={0} | all-to-all | bytes 2359296 | tf_op jit(solution)/shard_map/all_to_all | solution.py:15
  117.2 1.4 convolution_convert_fusion
  118.6 2.4 %reshape.121 = bf16[64,18,1024]{2,1,0:T(8,128)(2,1)} reshape(bf16[1152,1024]{1,0:T(8,128)(2,1)S(1)} %convolution_convert_fusion) | data formatting | bytes 4718592 | tf_op jit(solution)/shard_map/reshape | solution.py:132
  121.0 5.9 %all-to-all-start.5 = ((bf16[64,18,1024]{2,1,0:T(8,128)(2,1)}), bf16[64,18,1024]{2,1,0:T(8,128)(2,1)}, u32[]{:S(2)}, u32[]{:S(2)}) async-start(bf16[64,18,1024]{2,1,0:T(8,128)(2,1)} %reshape.121), calls=%async_computation.5 | async-start | bytes 6291456 | tf_op jit(solution)/shard_map/all_to_all | solution.py:133
  127.3 0.7 copy.87
  128.0 0.3 fusion.52
  128.3 1.5 fusion.18
  129.8 2.0 %all_gather.7 = bf16[64,512]{1,0:T(8,128)(2,1)} all-gather(bf16[64,256]{1,0:T(8,128)(2,1)S(1)} %fusion.18), channel_id=1, replica_groups=mesh['ep'=64,'tp'=2] {'tp'}, dimensions={1}, use_global_device_ids=true | all-gather | bytes 98304 | tf_op jit(solution)/shard_map/all_gather | solution.py:142
  131.8 0.8 pad_maximum_fusion.1
  132.6 36.9 %all-to-all-done.5 = bf16[64,18,1024]{2,1,0:T(8,128)(2,1)} async-done(((bf16[64,18,1024]{2,1,0:T(8,128)(2,1)}), bf16[64,18,1024]{2,1,0:T(8,128)(2,1)}, u32[]{:S(2)}, u32[]{:S(2)}) %all-to-all-start.5) | async-done | bytes 2359328 | tf_op jit(solution)/shard_map/all_to_all | solution.py:133
  169.4 2.9 %reshape.122 = bf16[1152,1024]{1,0:T(8,128)(2,1)S(1)} reshape(bf16[64,18,1024]{2,1,0:T(8,128)(2,1)} %all-to-all-done.5) | data formatting | bytes 4718592 | tf_op jit(solution)/shard_map/reshape | solution.py:133
  172.4 2.7 %gather_fusion = bf16[384,1024]{1,0:T(8,128)(2,1)} fusion(bf16[1152,1024]{1,0:T(8,128)(2,1)S(1)} %reshape.122, s32[1024]{0:T(1024)S(1)} %pad_clamp_fusion), kind=kCustom, calls=%fused_computation | custom fusion | bytes 1574400 | tf_op jit(solution)/shard_map/gather | solution.py:136
  175.1 1.3 reshape.138
  176.4 1.5 multiply_reduce_fusion
  177.9 2.2 %fusion.17 = bf16[64,1024]{1,0:T(8,128)(2,1)} fusion(bf16[64,512]{1,0:T(8,128)(2,1)} %all_gather.7, bf16[512,1024]{1,0:T(8,128)(2,1)} %param.40, f32[64,1024]{1,0:T(8,128)S(1)} %multiply_reduce_fusion, bf16[64,1024]{1,0:T(8,128)(2,1)S(1)} %fusion.15, f32[1024]{0:T(1024)S(1)} %copy-done.14), kind=kOutput, calls=%fused_computation.30 | convolution fusion | flops 67567616 | bytes 1642496 | tf_op jit(solution)/shard_map/dot_general | solution.py:25
  (62 shorter events, 1.3 us)
Async XLA Ops:
  0.6 116.6 %copy-start = (bf16[1,512,1024]{2,1,0:T(8,128)(2,1)S(1)}, bf16[1,512,1024]{2,1,0:T(8,128)(2,1)}, u32[]{:S(2)}) copy-start(bf16[1,512,1024]{2,1,0:T(8,128)(2,1)} %param.37) | copy-start | bytes 3145732
  0.6 7.0 %copy-start.5 = (bf16[64,3,1024]{2,0,1:T(8,128)(2,1)S(1)}, bf16[64,3,1024]{2,0,1:T(8,128)(2,1)}, u32[]{:S(2)}) copy-start(bf16[64,3,1024]{2,0,1:T(8,128)(2,1)} %param.22) | copy-start | bytes 1179652
  2.4 5.0 %all-to-all-start = ((bf16[2,64,1024]{2,1,0:T(8,128)(2,1)}), bf16[2,64,1024]{2,1,0:T(8,128)(2,1)S(1)}, u32[]{:S(2)}, u32[]{:S(2)}) async-start(bf16[2,64,1024]{2,1,0:T(8,128)(2,1)} %broadcast_in_dim.10), calls=%async_computation | async-start | bytes 524288 | tf_op jit(solution)/shard_map/all_to_all | solution.py:15
  7.4 4.3 %copy-start.19 = (bf16[8,128,128]{2,1,0:T(8,128)(2,1)S(1)}, bf16[8,128,128]{2,1,0:T(8,128)(2,1)}, u32[]{:S(2)}) copy-start(bf16[8,128,128]{2,1,0:T(8,128)(2,1)} %param.29) | copy-start | bytes 786436
  7.7 4.3 %copy-start.20 = (bf16[8,128,128]{2,1,0:T(8,128)(2,1)S(1)}, bf16[8,128,128]{2,1,0:T(8,128)(2,1)}, u32[]{:S(2)}) copy-start(bf16[8,128,128]{2,1,0:T(8,128)(2,1)} %param.28) | copy-start | bytes 786436
  7.7 4.5 %copy-start.16 = (f32[1024]{0:T(1024)S(1)}, f32[1024]{0:T(1024)}, u32[]{:S(2)}) copy-start(f32[1024]{0:T(1024)} %param.30) | copy-start | bytes 12292
  7.7 4.5 %copy-start.10 = (f32[64,1024]{1,0:T(8,128)S(1)}, f32[64,1024]{1,0:T(8,128)}, u32[]{:S(2)}) copy-start(f32[64,1024]{1,0:T(8,128)} %param.23) | copy-start | bytes 786436
  7.7 4.8 %copy-start.2 = (bf16[2048,1024]{1,0:T(8,128)(2,1)S(1)}, bf16[2048,1024]{1,0:T(8,128)(2,1)}, u32[]{:S(2)}) copy-start(bf16[2048,1024]{1,0:T(8,128)(2,1)} %param.26) | copy-start | bytes 12582916
  11.7 0.8 copy-start.11
  12.2 3.4 %copy-start.1 = (bf16[2048,1024]{1,0:T(8,128)(2,1)S(1)}, bf16[2048,1024]{1,0:T(8,128)(2,1)}, u32[]{:S(2)}) copy-start(bf16[2048,1024]{1,0:T(8,128)(2,1)} %param.31) | copy-start | bytes 12582916
  12.3 3.4 %copy-start.8 = (bf16[64,1024]{1,0:T(8,128)(2,1)S(1)}, bf16[64,1024]{1,0:T(8,128)(2,1)}, u32[]{:S(2)}) copy-start(bf16[64,1024]{1,0:T(8,128)(2,1)} %param.21) | copy-start | bytes 393220
  12.5 4.0 %copy-start.7 = (f32[64,1024]{1,0:T(8,128)}, f32[64,1024]{1,0:T(8,128)S(1)}, u32[]{:S(2)}) copy-start(f32[64,1024]{1,0:T(8,128)S(1)} %fusion.36) | copy-start | bytes 786436
  13.5 7.2 %copy-start.12 = (s32[64,6]{0,1:T(8,128)S(1)}, s32[64,6]{0,1:T(8,128)}, u32[]{:S(2)}) copy-start(s32[64,6]{0,1:T(8,128)} %param.33) | copy-start | bytes 4612
  15.6 9.4 %copy-start.13 = (f32[2048]{0:T(1024)S(1)}, f32[2048]{0:T(1024)}, u32[]{:S(2)}) copy-start(f32[2048]{0:T(1024)} %param.32) | copy-start | bytes 24580
  17.3 5.0 %all-to-all-start.1 = ((bf16[2,64,1024]{2,1,0:T(8,128)(2,1)}), bf16[2,64,1024]{2,1,0:T(8,128)(2,1)S(1)}, u32[]{:S(2)}, u32[]{:S(2)}) async-start(bf16[2,64,1024]{2,1,0:T(8,128)(2,1)} %broadcast_in_dim.11), calls=%async_computation.1 | async-start | bytes 524288 | tf_op jit(solution)/shard_map/all_to_all | solution.py:15
  25.2 0.7 copy-start.3
  104.7 4.4 %copy-start.17 = (bf16[1,2048,256]{2,1,0:T(8,128)(2,1)S(1)}, bf16[1,2048,256]{2,1,0:T(8,128)(2,1)}, u32[]{:S(2)}) copy-start(bf16[1,2048,256]{2,1,0:T(8,128)(2,1)} %param.35) | copy-start | bytes 3145732
  109.1 1.4 copy-start.18
  121.0 6.2 %copy-start.15 = (f32[64,6]{0,1:T(8,128)S(1)}, f32[64,6]{0,1:T(8,128)}, u32[]{:S(2)}) copy-start(f32[64,6]{0,1:T(8,128)} %param.34) | copy-start | bytes 4612
  121.0 6.9 %copy-start.4 = (bf16[64,2048]{1,0:T(8,128)(2,1)S(1)}, bf16[64,2048]{1,0:T(8,128)(2,1)}, u32[]{:S(2)}) copy-start(bf16[64,2048]{1,0:T(8,128)(2,1)} %copy-done.3) | copy-start | bytes 786436
  121.0 6.9 %copy-start.6 = (bf16[2048,256]{1,0:T(8,128)(2,1)S(1)}, bf16[2048,256]{1,0:T(8,128)(2,1)}, u32[]{:S(2)}) copy-start(bf16[2048,256]{1,0:T(8,128)(2,1)} %param.38) | copy-start | bytes 3145732
  121.0 48.4 %all-to-all-start.5 = ((bf16[64,18,1024]{2,1,0:T(8,128)(2,1)}), bf16[64,18,1024]{2,1,0:T(8,128)(2,1)}, u32[]{:S(2)}, u32[]{:S(2)}) async-start(bf16[64,18,1024]{2,1,0:T(8,128)(2,1)} %reshape.121), calls=%async_computation.5 | async-start | bytes 6291456 | tf_op jit(solution)/shard_map/all_to_all | solution.py:133
  127.0 4.8 %slice-start = ((bf16[64,3,1024]{2,0,1:T(8,128)(2,1)}), bf16[64,2,1024]{2,0,1:T(8,128)(2,1)S(1)}, s32[]{:S(2)}) async-start(bf16[64,3,1024]{2,0,1:T(8,128)(2,1)} %param.22), calls=%async_computation.6 | async-start | bytes 524288 | tf_op jit(solution)/shard_map/slice | solution.py:69
  127.0 4.8 %copy-start.9 = (bf16[64,1024]{1,0:T(8,128)(2,1)S(1)}, bf16[64,1024]{1,0:T(8,128)(2,1)}, u32[]{:S(2)}) copy-start(bf16[64,1024]{1,0:T(8,128)(2,1)} %get-tuple-element.18) | copy-start | bytes 393220
  175.1 2.8 %copy-start.14 = (f32[1024]{0:T(1024)S(1)}, f32[1024]{0:T(1024)}, u32[]{:S(2)}) copy-start(f32[1024]{0:T(1024)} %param.41) | copy-start | bytes 12292
